TPU v7x, 128 devices: a whole 4x4x4 slice. The times are simulated.
128 devices in a mesh: gr: 2 (over z_hi), fs: 32 (over z_lo, y, x), tp: 2 (over core).
Axes of the slice: x: 4, y: 4, z: 4 (z_hi: 2, z_lo: 2; z = z_hi * 2 + z_lo), core: 2. Of those that a mesh axis runs over, the one named last changes fastest.
Arguments:
- tokens: bfloat16 [4, 2048, 2048], P(('gr', 'tp')), may hold values from -6 to 6
- gate_master: float32 [3, 2048, 7168], P(None, 'fs', ('gr', 'tp')), may hold values from -0.125 to 0.125
- up_master: float32 [3, 2048, 7168], P(None, 'fs', ('gr', 'tp')), may hold values from -0.125 to 0.125
- down_master: float32 [3, 7168, 2048], P(None, 'fs', ('gr', 'tp')), may hold values from -0.0625 to 0.0625
- norm_gain: float32 [2048], P('fs'), may hold values from 0.1 to 1.9
- route: int32 [4, 2048, 2], P(('gr', 'tp')), may hold values from 0 to 2, all different within a row
- route_weight: float32 [4, 2048, 2], P(('gr', 'tp')), may hold values from 0.05 to 1
Outputs:
- gate_out: bfloat16 [3, 2048, 7168], P(None, None, 'fs')
- up_out: bfloat16 [3, 2048, 7168], P(None, None, 'fs')
- down_out: bfloat16 [3, 7168, 2048], P(None, 'fs')
- mixed: bfloat16 [4, 2048, 2048], P(('gr', 'tp'), 'fs')
Inputs may be any that keep to these rules, and one draw needn't show every extreme that they name: `route`: each token names two different experts; every expert is named by some token.
All inputs are finite; a program needn't handle non-finite values.
Results may differ from a plain program's by a relative error of at most 0.024.
Values may be sent and summed in bfloat16 or wider, within the bound.
No kernel may reach another device: no remote copies, remote signals or barrier semaphores. Data moves between devices by JAX's collectives and lax.ppermute only.
A program may use at most 192 MiB of HBM per device.

v0:
```python
import jax
import jax.numpy as jnp
from jax import lax
from jax.sharding import Mesh
from jax.sharding import PartitionSpec as P

FS = ("fs_0", "fs_1", "fs_2")


def reduced_to_own(blocks, axes, order):
    dims = [lax.axis_size(a) for a in axes]
    blocks = blocks.reshape(*dims, *blocks.shape[1:])
    blocks = blocks.transpose(*order, *range(len(axes), blocks.ndim))
    blocks = blocks.reshape(-1, *blocks.shape[len(axes) :])
    for k in order:
        blocks = lax.psum_scatter(blocks, axes[k], scatter_dimension=0, tiled=True)
    return blocks[0]


def split_up(array, dim, peers):
    dims = array.shape
    blocks = array.reshape(*dims[:dim], peers, dims[dim] // peers, *dims[dim + 1 :])
    return jnp.moveaxis(blocks, dim, 0)


def sum_by_axis_2(array, axes, order, dim):
    peers = lax.axis_size(axes)
    return reduced_to_own(split_up(array, dim, peers), axes, order)


def normalize(rows_in):
    values = rows_in.astype(jnp.float32)
    scaled = values * lax.rsqrt(jnp.mean(values * values, axis=-1, keepdims=True) + 1e-06)
    return scaled.astype(jnp.bfloat16)


def mixing(chosen, weights, experts):
    share = weights / jnp.sum(weights, axis=-1, keepdims=True)
    labels = jnp.arange(experts, dtype=jnp.int32)
    match = (chosen[:, :, None] == labels[None, None, :]).astype(jnp.float32)
    return jnp.sum(share[:, :, None] * match, axis=1)


def expert_term(normed, mix_column, gate_weight, up_weight, down_weight):
    gate_act = jnp.dot(normed, gate_weight, preferred_element_type=jnp.float32)
    up_act = jnp.dot(normed, up_weight, preferred_element_type=jnp.float32)
    hidden = (jax.nn.silu(gate_act) * up_act).astype(jnp.bfloat16)
    projected = jnp.dot(hidden, down_weight, preferred_element_type=jnp.float32)
    return mix_column * projected


def shards(tokens, gate_master, up_master, down_master, norm_gain, route, route_weight):
    scaled_gain = norm_gain[None, :, None]
    gate_local = (scaled_gain * gate_master).astype(jnp.bfloat16)
    up_local = (scaled_gain * up_master).astype(jnp.bfloat16)
    down_local = down_master.astype(jnp.bfloat16)
    experts = gate_local.shape[0]
    normed = normalize(tokens[0])
    combine = mixing(route[0], route_weight[0], experts)
    width = normed.shape[1]
    gate_rows, up_rows, down_out = (
        lax.all_gather(gate_local, ("gr", "tp"), axis=2, tiled=True),
        lax.all_gather(up_local, ("gr", "tp"), axis=2, tiled=True),
        lax.all_gather(down_local, ("gr", "tp"), axis=2, tiled=True),
    )
    gate_out, up_out = (
        lax.all_to_all(gate_rows, FS, split_axis=2, concat_axis=1, tiled=True),
        lax.all_to_all(up_rows, FS, split_axis=2, concat_axis=1, tiled=True),
    )
    own_rows = normed.shape[0] // lax.axis_size(FS)
    total = jnp.zeros((own_rows * lax.axis_size(FS), width), jnp.float32)
    for index in range(experts):
        total = total + expert_term(
            normed, combine[:, index : index + 1], gate_out[index], up_out[index], down_out[index]
        )
    summed = sum_by_axis_2(total.astype(jnp.bfloat16), FS, (1, 2, 0), 0).astype(jnp.float32)
    mixed = summed.astype(jnp.bfloat16)[None]
    return (gate_out, up_out, down_out, mixed)


def solution(mesh):
    split = Mesh(
        mesh.devices.reshape(mesh.shape["gr"], 2, 4, 4, mesh.shape["tp"]),
        ("gr", "fs_0", "fs_1", "fs_2", "tp"),
    )
    in_specs = (
        P(("gr", "tp"), None, None),
        P(None, FS, ("gr", "tp")),
        P(None, FS, ("gr", "tp")),
        P(None, FS, ("gr", "tp")),
        P(FS),
        P(("gr", "tp"), None, None),
        P(("gr", "tp"), None, None),
    )
    out_specs = (P(None, None, FS), P(None, None, FS), P(None, FS, None), P(("gr", "tp"), FS, None))
    return jax.shard_map(
        shards, mesh=split, in_specs=in_specs, out_specs=out_specs, check_vma=False
    )
```

profile of v0, /device:TPU:1, one launch (start us, length us, event | category | flops | bytes accessed | tf_op | source)
XLA Modules:
  0.0 390.9 jit_solution(5299467397481243480)
XLA Ops:
  7.2 0.0 all-gather.4.cloned.1.call-start
  7.2 3.1 multiply_convert_fusion
  10.3 0.0 all-gather.4.cloned.1.call-update
  10.3 0.0 all-gather.6.cloned.1.call-start
  10.4 0.7 all-gather.6.cloned.1.call-update
  11.1 33.5 %all-gather.4.cloned.1.call-done = bf16[3,64,7168]{2,1,0:T(8,128)(2,1)} async-done(((bf16[3,64,1792]{2,1,0:T(8,128)(2,1)}), bf16[3,64,7168]{2,1,0:T(8,128)(2,1)}) %all-gather.4.cloned.1.call-update) | async-done | bytes 2752528 | tf_op jit(solution)/shard_map/all_gather | solution.py:62
  44.5 10.1 %copy.41 = bf16[3,64,7168]{1,0,2:T(4,128)(2,1)} copy(bf16[3,64,7168]{2,1,0:T(8,128)(2,1)} %all-gather.4.cloned.1.call-done) | data formatting | bytes 5505024 | tf_op jit(solution)/shard_map/all_gather | solution.py:62
  54.6 12.6 %reshape.105 = bf16[32,2,21504]{2,1,0:T(2,128)(2,1)} reshape(bf16[7168,3,64]{2,1,0:T(4,128)(2,1)} %bitcast.55) | data formatting | bytes 5505024
  67.2 7.0 %all-to-all-start = ((bf16[32,2,21504]{2,1,0:T(2,128)(2,1)}), bf16[32,2,21504]{2,1,0:T(2,128)(2,1)S(1)}, u32[]{:S(2)}, u32[]{:S(2)}) async-start(bf16[32,2,21504]{2,1,0:T(2,128)(2,1)} %reshape.105), calls=%async_computation | async-start | bytes 5505024 | tf_op jit(solution)/shard_map/all_to_all | solution.py:67
  74.3 0.0 copy-start.2
  74.3 0.0 all-gather.8.cloned.1.call-start
  74.3 2.3 convert_element_type.47
  76.6 0.0 all-gather.8.cloned.1.call-update
  76.6 0.0 copy-done.2
  76.7 0.0 all-gather.6.cloned.1.call-done
  76.7 10.1 %copy.43 = bf16[3,64,7168]{1,0,2:T(4,128)(2,1)} copy(bf16[3,64,7168]{2,1,0:T(8,128)(2,1)} %all-gather.6.cloned.1.call-done) | data formatting | bytes 5505024 | tf_op jit(solution)/shard_map/all_gather | solution.py:63
  86.8 12.6 %reshape.107 = bf16[32,2,21504]{2,1,0:T(2,128)(2,1)} reshape(bf16[7168,3,64]{2,1,0:T(4,128)(2,1)} %bitcast.56) | data formatting | bytes 5505024
  99.4 0.0 copy-start.3
  99.4 9.2 %all-to-all-done = bf16[32,2,21504]{2,1,0:T(2,128)(2,1)S(1)} async-done(((bf16[32,2,21504]{2,1,0:T(2,128)(2,1)}), bf16[32,2,21504]{2,1,0:T(2,128)(2,1)S(1)}, u32[]{:S(2)}, u32[]{:S(2)}) %all-to-all-start) | async-done | bytes 2752544 | tf_op jit(solution)/shard_map/all_to_all | solution.py:67
  108.6 6.3 %all-to-all-start.1 = ((bf16[32,2,21504]{2,1,0:T(2,128)(2,1)}), bf16[32,2,21504]{2,1,0:T(2,128)(2,1)}, u32[]{:S(2)}, u32[]{:S(2)}) async-start(bf16[32,2,21504]{2,1,0:T(2,128)(2,1)} %reshape.107), calls=%async_computation.1 | async-start | bytes 5505024 | tf_op jit(solution)/shard_map/all_to_all | solution.py:68
  115.0 0.0 reduce-scatter.4.cloned.1.call-start
  115.0 0.0 copy-done.3
  115.0 0.1 fusion.20
  115.1 5.1 %fusion = f32[2048]{0:T(1024)S(1)} fusion(bf16[1,2048,2048]{2,1,0:T(8,128)(2,1)} %param.7), kind=kLoop, calls=%fused_computation.2 | loop fusion | flops 12580864 | bytes 8396800 | tf_op jit(solution)/shard_map/reduce_sum | solution.py:33
  120.3 8.0 %fusion.2 = bf16[2048,2048]{1,0:T(8,128)(2,1)} fusion(bf16[1,2048,2048]{2,1,0:T(8,128)(2,1)} %param.7, f32[2048]{0:T(1024)S(1)} %add_rsqrt_fusion), kind=kLoop, calls=%fused_computation.5 | loop fusion | flops 12582912 | bytes 16785408 | tf_op jit(solution)/shard_map/convert_element_type | solution.py:34
  128.3 8.7 %reshape.106 = bf16[7168,3,64]{2,1,0:T(4,128)(2,1)} reshape(bf16[32,2,21504]{2,1,0:T(2,128)(2,1)S(1)} %all-to-all-done) | data formatting | bytes 5505024
  136.9 10.7 %copy.42 = bf16[3,64,32,224]{3,1,2,0:T(8,128)(2,1)S(1)} copy(bf16[3,64,32,224]{1,0,3,2:T(4,128)(2,1)} %bitcast.57) | data formatting | bytes 5505024 | tf_op jit(solution)/shard_map/all_to_all | solution.py:67
  147.7 0.9 all-to-all-done.1
  148.6 12.5 %reshape.108 = bf16[7168,3,64]{2,1,0:T(4,128)(2,1)} reshape(bf16[32,2,21504]{2,1,0:T(2,128)(2,1)} %all-to-all-done.1) | data formatting | bytes 5505024
  161.0 11.4 %copy.44 = bf16[3,64,32,224]{3,1,2,0:T(8,128)(2,1)} copy(bf16[3,64,32,224]{1,0,3,2:T(4,128)(2,1)} %bitcast.58) | data formatting | bytes 5505024 | tf_op jit(solution)/shard_map/all_to_all | solution.py:68
  172.4 0.0 copy-start
  172.4 0.2 fusion.24
  172.6 1.7 copy-done
  174.3 0.0 slice-start
  174.3 1.8 fusion.25
  176.1 0.0 slice-start.1
  176.1 8.0 %fusion.27 = f32[2048,224]{0,1:T(8,128)} fusion(bf16[2048,2048]{1,0:T(8,128)(2,1)} %fusion.2, bf16[2048,224]{1,0:T(8,128)(2,1)S(1)} %bitcast.68), kind=kOutput, calls=%fused_computation.41 | convolution fusion | flops 1879048192 | bytes 11141120 | tf_op jit(solution)/shard_map/dot_general | solution.py:45
  184.1 0.0 slice-done
  184.1 0.0 slice-done.1
  184.1 4.0 %fusion.28 = f32[2048,224]{0,1:T(8,128)} fusion(bf16[2048,2048]{1,0:T(8,128)(2,1)S(1)} %bitcast.52, bf16[2048,224]{1,0:T(8,128)(2,1)S(1)} %bitcast.67), kind=kOutput, calls=%fused_computation.42 | convolution fusion | flops 1879048192 | bytes 11141120 | tf_op jit(solution)/shard_map/dot_general | solution.py:45
  188.1 4.0 %fusion.29 = f32[2048,224]{0,1:T(8,128)} fusion(bf16[2048,2048]{1,0:T(8,128)(2,1)S(1)} %bitcast.52, bf16[2048,224]{1,0:T(8,128)(2,1)S(1)} %bitcast.66), kind=kOutput, calls=%fused_computation.43 | convolution fusion | flops 1879048192 | bytes 11141120 | tf_op jit(solution)/shard_map/dot_general | solution.py:45
  192.1 0.0 all-gather.8.cloned.1.call-done
  192.1 15.3 %fusion.7 = f32[2048,2048]{1,0:T(8,128)} fusion(bf16[2048,2048]{1,0:T(8,128)(2,1)} %fusion.2, bf16[2048,224]{1,0:T(8,128)(2,1)} %bitcast.64, f32[2048,224]{0,1:T(8,128)} %fusion.27, bf16[3,224,2048]{2,1,0:T(8,128)(2,1)} %all-gather.8.cloned.1.call-done), kind=kOutput, calls=%fused_computation.13 | convolution fusion | flops 3760848896 | bytes 28966912 | tf_op jit(solution)/shard_map/dot_general | solution.py:48
  207.4 15.5 %fusion.6 = f32[2048,2048]{1,0:T(8,128)} fusion(bf16[2048,2048]{1,0:T(8,128)(2,1)} %fusion.2, bf16[2048,224]{1,0:T(8,128)(2,1)} %bitcast.63, f32[2048,224]{0,1:T(8,128)} %fusion.28, bf16[3,224,2048]{2,1,0:T(8,128)(2,1)} %all-gather.8.cloned.1.call-done), kind=kOutput, calls=%fused_computation.12 | convolution fusion | flops 3760848896 | bytes 28966912 | tf_op jit(solution)/shard_map/dot_general | solution.py:48
  222.9 19.2 %add_convert_fusion = bf16[2048,2048]{1,0:T(8,128)(2,1)} fusion(f32[2048,2048]{1,0:T(8,128)} %fusion.6, f32[2048,2048]{1,0:T(8,128)} %fusion.7, f32[2048]{0:T(1024)S(1)} %bitcast.70, f32[2048]{0:T(1024)S(1)} %bitcast.71, f32[2048]{0:T(1024)S(1)} %bitcast.69, bf16[3,224,2048]{2,1,0:T(8,128)(2,1)} %all-gather.8.cloned.1.call-done, ...), kind=kOutput, calls=%fused_computation.4 | convolution fusion | flops 3786014720 | bytes 54157312 | tf_op jit(solution)/shard_map/dot_general | solution.py:48
  242.0 8.3 %copy.45 = bf16[4,4,2,64,2048]{4,3,2,1,0:T(8,128)(2,1)} copy(bf16[4,4,2,64,2048]{4,3,1,0,2:T(8,128)(2,1)} %bitcast.54) | data formatting | bytes 16777216 | tf_op jit(solution)/shard_map/transpose | solution.py:13
  250.3 0.0 reduce-scatter.4.cloned.1.call-update
  250.3 0.0 reduce-scatter.6.cloned.1.call-start
  250.4 80.8 %reduce-scatter.4.cloned.1.call-done = bf16[8,64,2048]{2,1,0:T(8,128)(2,1)} async-done(((bf16[32,64,2048]{2,1,0:T(8,128)(2,1)}), bf16[8,64,2048]{2,1,0:T(8,128)(2,1)}) %reduce-scatter.4.cloned.1.call-update) | async-done | bytes 2097168 | tf_op jit(solution)/shard_map/reduce_scatter | solution.py:16
  331.2 0.0 reduce-scatter.6.cloned.1.call-update
  331.2 0.0 reduce-scatter.8.cloned.1.call-start
  331.3 31.6 %reduce-scatter.6.cloned.1.call-done = bf16[2,64,2048]{2,1,0:T(8,128)(2,1)} async-done(((bf16[8,64,2048]{2,1,0:T(8,128)(2,1)}), bf16[2,64,2048]{2,1,0:T(8,128)(2,1)}) %reduce-scatter.6.cloned.1.call-update) | async-done | bytes 524304 | tf_op jit(solution)/shard_map/reduce_scatter | solution.py:16
  362.9 0.0 reduce-scatter.8.cloned.1.call-update
  362.9 2.7 copy.46
  365.6 0.0 copy-start.1
  365.6 4.7 %copy.47 = bf16[3,2048,224]{1,2,0:T(8,128)(2,1)} copy(bf16[3,2048,224]{2,1,0:T(8,128)(2,1)} %bitcast.61) | data formatting | bytes 5505024
  370.3 12.2 %reduce-scatter.8.cloned.1.call-done = bf16[1,64,2048]{2,1,0:T(8,128)(2,1)} async-done(((bf16[2,64,2048]{2,1,0:T(8,128)(2,1)}), bf16[1,64,2048]{2,1,0:T(8,128)(2,1)}) %reduce-scatter.8.cloned.1.call-update) | async-done | bytes 262160 | tf_op jit(solution)/shard_map/reduce_scatter | solution.py:16
  382.5 0.0 copy-done.1
  382.5 1.5 copy.49
  (5 shorter events, 0.1 us)
Async XLA Ops:
  7.2 37.4 %all-gather.4.cloned.1.call-start = ((), (), s32[]{:S(2)}) async-start(), calls=%async_computation.5 | async-start | bytes 3440640 | tf_op jit(solution)/shard_map/all_gather | solution.py:62
  10.3 66.4 %all-gather.6.cloned.1.call-start = ((), (), s32[]{:S(2)}) async-start(), calls=%async_computation.6 | async-start | bytes 3440640 | tf_op jit(solution)/shard_map/all_gather | solution.py:63
  67.2 41.4 %all-to-all-start = ((bf16[32,2,21504]{2,1,0:T(2,128)(2,1)}), bf16[32,2,21504]{2,1,0:T(2,128)(2,1)S(1)}, u32[]{:S(2)}, u32[]{:S(2)}) async-start(bf16[32,2,21504]{2,1,0:T(2,128)(2,1)} %reshape.105), calls=%async_computation | async-start | bytes 5505024 | tf_op jit(solution)/shard_map/all_to_all | solution.py:67
  74.3 2.4 copy-start.2
  74.3 117.9 %all-gather.8.cloned.1.call-start = ((), (), s32[]{:S(2)}) async-start(), calls=%async_computation.7 | async-start | bytes 3440640 | tf_op jit(solution)/shard_map/all_gather | solution.py:64
  99.4 15.6 %copy-start.3 = (s32[1,2048,2]{1,2,0:T(2,128)S(1)}, s32[1,2048,2]{1,2,0:T(2,128)}, u32[]{:S(2)}) copy-start(s32[1,2048,2]{1,2,0:T(2,128)} %param.12) | copy-start | bytes 49156
  108.6 39.9 %all-to-all-start.1 = ((bf16[32,2,21504]{2,1,0:T(2,128)(2,1)}), bf16[32,2,21504]{2,1,0:T(2,128)(2,1)}, u32[]{:S(2)}, u32[]{:S(2)}) async-start(bf16[32,2,21504]{2,1,0:T(2,128)(2,1)} %reshape.107), calls=%async_computation.1 | async-start | bytes 5505024 | tf_op jit(solution)/shard_map/all_to_all | solution.py:68
  115.0 216.3 %reduce-scatter.4.cloned.1.call-start = ((), (), s32[]{:S(2)}) async-start(), calls=%async_computation.8 | async-start | bytes 10485760 | tf_op jit(solution)/shard_map/reduce_scatter | solution.py:16
  172.4 1.9 copy-start
  174.3 9.8 %slice-start = ((s8[8388608]{0:T(1024)(128)(4,1)}), s8[4194304]{0:T(1024)(128)(4,1)S(1)}, s32[]{:S(2)}) async-start(s8[8388608]{0:T(1024)(128)(4,1)} %bitcast.51), calls=%async_computation.11 | async-start | bytes 8388608
  176.1 8.0 %slice-start.1 = ((s8[8388608]{0:T(1024)(128)(4,1)}), s8[4194304]{0:T(1024)(128)(4,1)S(1)}, s32[]{:S(2)}) async-start(s8[8388608]{0:T(1024)(128)(4,1)} %bitcast.51), calls=%async_computation.12 | async-start | bytes 8388608
  250.3 112.5 %reduce-scatter.6.cloned.1.call-start = ((), (), s32[]{:S(2)}) async-start(), calls=%async_computation.9 | async-start | bytes 2621440 | tf_op jit(solution)/shard_map/reduce_scatter | solution.py:16
  331.2 51.3 %reduce-scatter.8.cloned.1.call-start = ((), (), s32[]{:S(2)}) async-start(), calls=%async_computation.10 | async-start | bytes 786432 | tf_op jit(solution)/shard_map/reduce_scatter | solution.py:16
  365.6 16.9 %copy-start.1 = (bf16[3,224,2048]{2,1,0:T(8,128)(2,1)S(1)}, bf16[3,224,2048]{2,1,0:T(8,128)(2,1)}, u32[]{:S(2)}) copy-start(bf16[3,224,2048]{2,1,0:T(8,128)(2,1)} %all-gather.8.cloned.1.call-done) | copy-start | bytes 8257540
Sparse Core Ops, SparseCore 0:
  10.4 34.0 all-gather.3
  46.8 29.6 all-gather.5
  78.1 74.4 all-gather.7
  250.5 80.7 reduce-scatter.3
  333.5 29.3 reduce-scatter.5
  365.6 16.8 reduce-scatter.7
where the time goes:
time: 393 us; the launch traced here: 391 us
  waiting for transfers between devices  169 us (43%)
  local copies, waits for them, and re-layouts  110 us (28%)
  matrix products  65.9 us (17%)
  other arithmetic  18.6 us (5%)
  between operations  14.2 us (4%)
  starting transfers between devices  13.6 us (3%)
    reduce_scatter x3, waiting for transfers between devices, reduced_to_own(): blocks = lax.psum_scatter(blocks, axes[k], scatter_dimension=0, tiled=True)  125 us
    unnamed x19, local copies, waits for them, and re-layouts  57 us
    dot_general x3, matrix products, expert_term(): projected = jnp.dot(hidden, down_weight, preferred_element_type=jnp.float32)  49.9 us
    all_gather x1, waiting for transfers between devices, shards(): lax.all_gather(gate_local, ('gr', 'tp'), axis=2, tiled=True)  33.5 us
    dot_general x3, matrix products, expert_term(): gate_act = jnp.dot(normed, gate_weight, preferred_element_type=jnp.float32)  16 us
    all_to_all x1, local copies, waits for them, and re-layouts, shards(): lax.all_to_all(up_rows, FS, split_axis=2, concat_axis=1, tiled=True)  11.4 us
    all_to_all x1, local copies, waits for them, and re-layouts, shards(): lax.all_to_all(gate_rows, FS, split_axis=2, concat_axis=1, tiled=True)  10.7 us
    all_gather x1, local copies, waits for them, and re-layouts, shards(): lax.all_gather(up_local, ('gr', 'tp'), axis=2, tiled=True)  10.1 us
  transfers between devices with their start and end apart: 8, of which 6 were waited for; matrix products, arithmetic and copies ran while one was open for 33% of the time, Pallas kernels for 0%

commit v1 on v0

--- a/solution.py
+++ b/solution.py
@@ -64,7 +64,10 @@
         lax.all_gather(down_local, ("gr", "tp"), axis=2, tiled=True),
     )
     gate_out, up_out = (
-        lax.all_to_all(gate_rows, FS, split_axis=2, concat_axis=1, tiled=True),
+        jnp.concatenate(
+            lax.all_to_all(jnp.stack(jnp.split(gate_rows, lax.axis_size(FS), axis=2)), FS, 0, 0),
+            axis=1,
+        ),
         lax.all_to_all(up_rows, FS, split_axis=2, concat_axis=1, tiled=True),
     )
     own_rows = normed.shape[0] // lax.axis_size(FS)

time: 393 us -> 383 us (0.975)
  waiting for transfers between devices: 169 us -> 159 us
    all_gather x1, waiting for transfers between devices: 0.02 us -> 32.4 us  [shards(): lax.all_gather(up_local, ('gr', 'tp'), axis=2, tiled=True)]
    all_gather x1, waiting for transfers between devices: 33.5 us -> 2.23 us  [shards(): lax.all_gather(gate_local, ('gr', 'tp'), axis=2, tiled=True)]
    unnamed x19 -> x54, local copies, waits for them, and re-layouts: 57 us -> 76 us
    all_to_all x1 -> x0, local copies, waits for them, and re-layouts: 10.7 us -> none  [shards(): lax.all_to_all(gate_rows, FS, split_axis=2, concat_axis=1, tiled=True)]
    all_gather x1 -> x0, local copies, waits for them, and re-layouts: 10.1 us -> none  [shards(): lax.all_gather(gate_local, ('gr', 'tp'), axis=2, tiled=True)]
    all_to_all x1, waiting for transfers between devices: 9.23 us -> 1.97 us  [shards(): lax.all_to_all(jnp.stack(jnp.split(gate_rows, lax.axis_size(FS), axis=2))...]
where the time goes in v1:
time: 383 us; the launch traced here: 381 us
  waiting for transfers between devices  159 us (42%)
  local copies, waits for them, and re-layouts  110 us (29%)
  matrix products  65.9 us (17%)
  other arithmetic  17.4 us (5%)
  starting transfers between devices  14.2 us (4%)
  between operations  14.2 us (4%)
    reduce_scatter x3, waiting for transfers between devices, reduced_to_own(): blocks = lax.psum_scatter(blocks, axes[k], scatter_dimension=0, tiled=True)  122 us
    unnamed x54, local copies, waits for them, and re-layouts  76 us
    dot_general x3, matrix products, expert_term(): projected = jnp.dot(hidden, down_weight, preferred_element_type=jnp.float32)  49.9 us
    all_gather x1, waiting for transfers between devices, shards(): lax.all_gather(up_local, ('gr', 'tp'), axis=2, tiled=True)  32.4 us
    dot_general x3, matrix products, expert_term(): gate_act = jnp.dot(normed, gate_weight, preferred_element_type=jnp.float32)  16 us
    all_to_all x1, local copies, waits for them, and re-layouts, shards(): lax.all_to_all(up_rows, FS, split_axis=2, concat_axis=1, tiled=True)  11.3 us
    all_gather x1, local copies, waits for them, and re-layouts, shards(): lax.all_gather(up_local, ('gr', 'tp'), axis=2, tiled=True)  10 us
    transpose x1, local copies, waits for them, and re-layouts, reduced_to_own(): blocks = blocks.transpose(*order, *range(len(axes), blocks.ndim))  8.28 us
  transfers between devices with their start and end apart: 8, of which 6 were waited for; matrix products, arithmetic and copies ran while one was open for 33% of the time, Pallas kernels for 0%

profile of v1, /device:TPU:1, one launch (start us, length us, event | category | flops | bytes accessed | tf_op | source)
XLA Modules:
  0.0 381.5 jit_solution(254166681760322126)
XLA Ops:
  7.2 3.2 multiply_convert_fusion
  10.5 0.7 all-gather.4.cloned.1.call-update
  11.2 1.0 convert_element_type.47
  12.3 32.4 %all-gather.6.cloned.1.call-done = bf16[3,64,7168]{2,1,0:T(8,128)(2,1)} async-done(((bf16[3,64,1792]{2,1,0:T(8,128)(2,1)}), bf16[3,64,7168]{2,1,0:T(8,128)(2,1)}) %all-gather.6.cloned.1.call-update) | async-done | bytes 2752528 | tf_op jit(solution)/shard_map/all_gather | solution.py:63
  44.6 10.0 %copy.53 = bf16[3,64,7168]{1,0,2:T(4,128)(2,1)} copy(bf16[3,64,7168]{2,1,0:T(8,128)(2,1)} %all-gather.6.cloned.1.call-done) | data formatting | bytes 5505024 | tf_op jit(solution)/shard_map/all_gather | solution.py:63
  54.7 12.6 %reshape.113 = bf16[32,2,21504]{2,1,0:T(2,128)(2,1)} reshape(bf16[7168,3,64]{2,1,0:T(4,128)(2,1)} %bitcast.179) | data formatting | bytes 5505024
  67.3 7.0 %all-to-all-start.1 = ((bf16[32,2,21504]{2,1,0:T(2,128)(2,1)}), bf16[32,2,21504]{2,1,0:T(2,128)(2,1)S(1)}, u32[]{:S(2)}, u32[]{:S(2)}) async-start(bf16[32,2,21504]{2,1,0:T(2,128)(2,1)} %reshape.113), calls=%async_computation.1 | async-start | bytes 5505024 | tf_op jit(solution)/shard_map/all_to_all | solution.py:71
  74.3 2.2 all-gather.4.cloned.1.call-done
  76.6 1.7 fusion.51
  78.3 1.6 fusion.50
  79.9 1.6 fusion.49
  81.6 1.6 fusion.48
  83.2 1.5 fusion.47
  84.7 1.6 fusion.46
  86.4 1.7 fusion.45
  88.0 1.7 fusion.44
  89.7 1.5 fusion.43
  91.2 1.6 fusion.42
  92.9 1.6 fusion.41
  94.5 1.6 fusion.40
  96.1 1.5 fusion.39
  97.7 1.6 fusion.38
  99.3 1.6 fusion.37
  101.0 1.6 fusion.36
  102.6 0.6 fusion.35
  103.3 0.7 fusion.34
  104.0 0.7 fusion.33
  104.7 0.7 fusion.32
  105.5 0.7 fusion.31
  106.1 0.7 fusion.30
  106.8 0.7 fusion.29
  107.6 0.7 fusion.28
  108.3 0.6 fusion.27
  109.0 0.7 fusion.26
  109.7 0.7 fusion.25
  110.4 0.7 fusion.24
  111.2 0.6 fusion.23
  111.8 0.7 fusion.22
  112.5 0.7 fusion.21
  113.3 0.7 fusion.20
  114.0 1.5 copy-done.2
  115.6 6.9 %all-to-all-start = ((bf16[32,3,64,224]{3,2,1,0:T(8,128)(2,1)}), bf16[32,3,64,224]{3,2,1,0:T(8,128)(2,1)S(1)}, u32[]{:S(2)}, u32[]{:S(2)}) async-start(bf16[32,3,64,224]{3,2,1,0:T(8,128)(2,1)} %fusion.20), calls=%async_computation | async-start | bytes 6291456 | tf_op jit(solution)/shard_map/all_to_all | solution.py:68
  122.6 5.1 %fusion = f32[2048]{0:T(1024)S(1)} fusion(bf16[1,2048,2048]{2,1,0:T(8,128)(2,1)} %param.7), kind=kLoop, calls=%fused_computation.2 | loop fusion | flops 12580864 | bytes 8396800 | tf_op jit(solution)/shard_map/reduce_sum | solution.py:33
  127.7 8.0 %fusion.2 = bf16[2048,2048]{1,0:T(8,128)(2,1)} fusion(bf16[1,2048,2048]{2,1,0:T(8,128)(2,1)} %param.7, f32[2048]{0:T(1024)S(1)} %add_rsqrt_fusion), kind=kLoop, calls=%fused_computation.5 | loop fusion | flops 12582912 | bytes 16785408 | tf_op jit(solution)/shard_map/convert_element_type | solution.py:34
  135.8 12.4 %reshape.114 = bf16[7168,3,64]{2,1,0:T(4,128)(2,1)} reshape(bf16[32,2,21504]{2,1,0:T(2,128)(2,1)} %copy-done.2) | data formatting | bytes 5505024
  148.2 11.3 %copy.54 = bf16[3,64,32,224]{3,1,2,0:T(8,128)(2,1)} copy(bf16[3,64,32,224]{1,0,3,2:T(4,128)(2,1)} %bitcast.180) | data formatting | bytes 5505024 | tf_op jit(solution)/shard_map/all_to_all | solution.py:71
  159.6 2.0 all-to-all-done
  161.5 0.2 fusion.56
  161.7 1.7 copy-done
  163.4 1.8 fusion.57
  165.3 8.0 %fusion.60 = f32[2048,224]{0,1:T(8,128)} fusion(bf16[2048,2048]{1,0:T(8,128)(2,1)} %fusion.2, bf16[2048,224]{1,0:T(8,128)(2,1)S(1)} %bitcast.191), kind=kOutput, calls=%fused_computation.106 | convolution fusion | flops 1879048192 | bytes 11141120 | tf_op jit(solution)/shard_map/dot_general | solution.py:45
  173.2 4.0 %fusion.59 = f32[2048,224]{0,1:T(8,128)} fusion(bf16[2048,2048]{1,0:T(8,128)(2,1)S(1)} %bitcast.176, bf16[2048,224]{1,0:T(8,128)(2,1)S(1)} %bitcast.190), kind=kOutput, calls=%fused_computation.105 | convolution fusion | flops 1879048192 | bytes 11141120 | tf_op jit(solution)/shard_map/dot_general | solution.py:45
  177.3 4.0 %fusion.61 = f32[2048,224]{0,1:T(8,128)} fusion(bf16[2048,2048]{1,0:T(8,128)(2,1)S(1)} %bitcast.176, bf16[2048,224]{1,0:T(8,128)(2,1)S(1)} %bitcast.189), kind=kOutput, calls=%fused_computation.107 | convolution fusion | flops 1879048192 | bytes 11141120 | tf_op jit(solution)/shard_map/dot_general | solution.py:45
  181.3 15.2 %fusion.6 = f32[2048,2048]{1,0:T(8,128)} fusion(bf16[2048,2048]{1,0:T(8,128)(2,1)} %fusion.2, bf16[2048,224]{1,0:T(8,128)(2,1)} %bitcast.187, f32[2048,224]{0,1:T(8,128)} %fusion.60, bf16[3,224,2048]{2,1,0:T(8,128)(2,1)} %all-gather.8.cloned.1.call-done), kind=kOutput, calls=%fused_computation.12 | convolution fusion | flops 3760848896 | bytes 28966912 | tf_op jit(solution)/shard_map/dot_general | solution.py:48
  196.5 15.5 %fusion.7 = f32[2048,2048]{1,0:T(8,128)} fusion(bf16[2048,2048]{1,0:T(8,128)(2,1)} %fusion.2, bf16[2048,224]{1,0:T(8,128)(2,1)} %bitcast.186, f32[2048,224]{0,1:T(8,128)} %fusion.59, bf16[3,224,2048]{2,1,0:T(8,128)(2,1)} %all-gather.8.cloned.1.call-done), kind=kOutput, calls=%fused_computation.13 | convolution fusion | flops 3760848896 | bytes 28966912 | tf_op jit(solution)/shard_map/dot_general | solution.py:48
  212.0 19.2 %add_convert_fusion = bf16[2048,2048]{1,0:T(8,128)(2,1)} fusion(f32[2048,2048]{1,0:T(8,128)} %fusion.6, f32[2048,2048]{1,0:T(8,128)} %fusion.7, f32[2048]{0:T(1024)S(1)} %bitcast.193, f32[2048]{0:T(1024)S(1)} %bitcast.194, f32[2048]{0:T(1024)S(1)} %bitcast.192, bf16[3,224,2048]{2,1,0:T(8,128)(2,1)} %all-gather.8.cloned.1.call-done, ...), kind=kOutput, calls=%fused_computation.4 | convolution fusion | flops 3786014720 | bytes 54157312 | tf_op jit(solution)/shard_map/dot_general | solution.py:48
  231.2 8.3 %copy.55 = bf16[4,4,2,64,2048]{4,3,2,1,0:T(8,128)(2,1)} copy(bf16[4,4,2,64,2048]{4,3,1,0,2:T(8,128)(2,1)} %bitcast.178) | data formatting | bytes 16777216 | tf_op jit(solution)/shard_map/transpose | solution.py:13
  239.5 80.2 %reduce-scatter.4.cloned.1.call-done = bf16[8,64,2048]{2,1,0:T(8,128)(2,1)} async-done(((bf16[32,64,2048]{2,1,0:T(8,128)(2,1)}), bf16[8,64,2048]{2,1,0:T(8,128)(2,1)}) %reduce-scatter.4.cloned.1.call-update) | async-done | bytes 2097168 | tf_op jit(solution)/shard_map/reduce_scatter | solution.py:16
  319.7 31.6 %reduce-scatter.6.cloned.1.call-done = bf16[2,64,2048]{2,1,0:T(8,128)(2,1)} async-done(((bf16[8,64,2048]{2,1,0:T(8,128)(2,1)}), bf16[2,64,2048]{2,1,0:T(8,128)(2,1)}) %reduce-scatter.6.cloned.1.call-update) | async-done | bytes 524304 | tf_op jit(solution)/shard_map/reduce_scatter | solution.py:16
  351.3 1.9 copy.52
  353.2 4.7 %copy.56 = bf16[3,2048,224]{1,2,0:T(8,128)(2,1)} copy(bf16[3,2048,224]{2,1,0:T(8,128)(2,1)} %bitcast.185) | data formatting | bytes 5505024
  357.9 2.7 copy.57
  360.6 10.4 %reduce-scatter.8.cloned.1.call-done = bf16[1,64,2048]{2,1,0:T(8,128)(2,1)} async-done(((bf16[2,64,2048]{2,1,0:T(8,128)(2,1)}), bf16[1,64,2048]{2,1,0:T(8,128)(2,1)}) %reduce-scatter.8.cloned.1.call-update) | async-done | bytes 262160 | tf_op jit(solution)/shard_map/reduce_scatter | solution.py:16
  371.0 3.7 copy.90
  (35 shorter events, 0.5 us)
Async XLA Ops:
  7.2 4.1 %copy-start.4 = (f32[3,224,512]{2,1,0:T(8,128)S(1)}, f32[3,224,512]{2,1,0:T(8,128)}, u32[]{:S(2)}) copy-start(f32[3,224,512]{2,1,0:T(8,128)} %param.10) | copy-start | bytes 4128772
  7.2 5.0 %copy-start.5 = (f32[1,2048,2]{1,2,0:T(2,128)S(1)}, f32[1,2048,2]{1,2,0:T(2,128)}, u32[]{:S(2)}) copy-start(f32[1,2048,2]{1,2,0:T(2,128)} %param.13) | copy-start | bytes 49156
  7.2 37.5 %all-gather.6.cloned.1.call-start = ((), (), s32[]{:S(2)}) async-start(), calls=%async_computation.6 | async-start | bytes 3440640 | tf_op jit(solution)/shard_map/all_gather | solution.py:63
  10.4 66.2 %all-gather.4.cloned.1.call-start = ((), (), s32[]{:S(2)}) async-start(), calls=%async_computation.5 | async-start | bytes 3440640 | tf_op jit(solution)/shard_map/all_gather | solution.py:62
  11.2 170.1 %all-gather.8.cloned.1.call-start = ((), (), s32[]{:S(2)}) async-start(), calls=%async_computation.7 | async-start | bytes 3440640 | tf_op jit(solution)/shard_map/all_gather | solution.py:64
  67.3 46.7 %all-to-all-start.1 = ((bf16[32,2,21504]{2,1,0:T(2,128)(2,1)}), bf16[32,2,21504]{2,1,0:T(2,128)(2,1)S(1)}, u32[]{:S(2)}, u32[]{:S(2)}) async-start(bf16[32,2,21504]{2,1,0:T(2,128)(2,1)} %reshape.113), calls=%async_computation.1 | async-start | bytes 5505024 | tf_op jit(solution)/shard_map/all_to_all | solution.py:71
  76.6 26.0 %copy-start.3 = (bf16[3,64,7168]{2,1,0:T(8,128)(2,1)S(1)}, bf16[3,64,7168]{2,1,0:T(8,128)(2,1)}, u32[]{:S(2)}) copy-start(bf16[3,64,7168]{2,1,0:T(8,128)(2,1)} %all-gather.4.cloned.1.call-done) | copy-start | bytes 8257540
  114.0 8.5 %copy-start.6 = (s32[1,2048,2]{1,2,0:T(2,128)S(1)}, s32[1,2048,2]{1,2,0:T(2,128)}, u32[]{:S(2)}) copy-start(s32[1,2048,2]{1,2,0:T(2,128)} %param.12) | copy-start | bytes 49156
  114.0 1.5 copy-start.2
  115.6 46.0 %all-to-all-start = ((bf16[32,3,64,224]{3,2,1,0:T(8,128)(2,1)}), bf16[32,3,64,224]{3,2,1,0:T(8,128)(2,1)S(1)}, u32[]{:S(2)}, u32[]{:S(2)}) async-start(bf16[32,3,64,224]{3,2,1,0:T(8,128)(2,1)} %fusion.20), calls=%async_computation | async-start | bytes 6291456 | tf_op jit(solution)/shard_map/all_to_all | solution.py:68
  122.5 197.2 %reduce-scatter.4.cloned.1.call-start = ((), (), s32[]{:S(2)}) async-start(), calls=%async_computation.8 | async-start | bytes 10485760 | tf_op jit(solution)/shard_map/reduce_scatter | solution.py:16
  161.5 1.9 copy-start
  163.4 9.8 %slice-start = ((s8[8388608]{0:T(1024)(128)(4,1)}), s8[4194304]{0:T(1024)(128)(4,1)S(1)}, s32[]{:S(2)}) async-start(s8[8388608]{0:T(1024)(128)(4,1)} %bitcast.175), calls=%async_computation.11 | async-start | bytes 8388608
  165.3 8.0 %slice-start.1 = ((s8[8388608]{0:T(1024)(128)(4,1)}), s8[4194304]{0:T(1024)(128)(4,1)S(1)}, s32[]{:S(2)}) async-start(s8[8388608]{0:T(1024)(128)(4,1)} %bitcast.175), calls=%async_computation.12 | async-start | bytes 8388608
  239.5 111.8 %reduce-scatter.6.cloned.1.call-start = ((), (), s32[]{:S(2)}) async-start(), calls=%async_computation.9 | async-start | bytes 2621440 | tf_op jit(solution)/shard_map/reduce_scatter | solution.py:16
  319.7 51.3 %reduce-scatter.8.cloned.1.call-start = ((), (), s32[]{:S(2)}) async-start(), calls=%async_computation.10 | async-start | bytes 786432 | tf_op jit(solution)/shard_map/reduce_scatter | solution.py:16
  353.2 4.7 %copy-start.1 = (bf16[3,64,32,224]{3,1,2,0:T(8,128)(2,1)S(1)}, bf16[3,64,32,224]{3,1,2,0:T(8,128)(2,1)}, u32[]{:S(2)}) copy-start(bf16[3,64,32,224]{3,1,2,0:T(8,128)(2,1)} %copy.54) | copy-start | bytes 8257540
Sparse Core Ops, SparseCore 0:
  10.5 34.0 all-gather.5
  46.9 29.6 all-gather.3
  78.3 44.9 all-gather.7
  239.6 80.0 reduce-scatter.3
  321.9 29.3 reduce-scatter.5
  354.1 16.8 reduce-scatter.7
